TPU v7x, 32 devices: a whole 2x2x4 slice. The times are simulated.
32 devices in a mesh: fs: 4 (over z), rep: 4 (over y, x), tp: 2 (over core).
Axes of the slice: x: 2, y: 2, z: 4, core: 2. Of those that a mesh axis runs over, the one named last changes fastest.
Arguments:
- normed: bfloat16 [10240, 2048], P(('fs', 'rep')), may hold values from -150 to 150
- rec_cot: bfloat16 [10240, 2048], P(('fs', 'rep'), 'tp'), may hold values from -1.4823177 to 1.4823177
- conv_out: bfloat16 [10240, 2048], P(('fs', 'rep'), 'tp'), may hold values from -6 to 6
- gate_cot: bfloat16 [10240, 2048], P(('fs', 'rep'), 'tp'), may hold values from -0.05908203 to 0.05908203
- rec_weight: float32 [2048, 2048], P('fs', 'tp'), may hold values from -0.125 to 0.125
- rec_moment: float32 [2048, 2048], P('fs', 'tp'), may hold values from -6 to 6
- rec_right: bfloat16 [2048, 256], P('tp'), may hold values from -1 to 2
- gate_weight: float32 [8, 256, 256], P('tp', 'fs'), may hold values from -0.375 to 0.375
- gate_moment: float32 [8, 256, 256], P('tp', 'fs'), may hold values from -6 to 6
- gate_left: bfloat16 [8, 256, 256], P('tp', 'fs'), may hold values from -1 to 2
- gate_right: bfloat16 [8, 256, 256], P('tp'), may hold values from -1 to 2
Outputs:
- rec_weight_new: float32 [2048, 2048], P('fs', 'tp')
- rec_moment_new: float32 [2048, 2048], P('fs', 'tp')
- rec_step: float32 [2048, 2048], P('fs', 'tp')
- rec_copy: bfloat16 [2048, 2048], P('fs', 'tp')
- gate_weight_new: float32 [8, 256, 256], P('tp', 'fs')
- gate_moment_new: float32 [8, 256, 256], P('tp', 'fs')
- gate_step: float32 [8, 256, 256], P('tp', 'fs')
- gate_copy: bfloat16 [8, 256, 256], P('tp', 'fs')
All inputs are finite; a program needn't handle non-finite values.
Results may differ from a plain program's by a relative error of at most 0.001.
Values sent between devices are 32-bit elements; how exact they have to be, the bound alone decides.
A program may use at most 64 MiB of HBM per device.

v0:
```python
import jax
import jax.numpy as jnp
from jax import lax
from jax.sharding import PartitionSpec as P

BETA = 0.9
LEARN_RATE = 0.02
EPSILON = 1e-06


def precondition_right(gradient, factor):
    row_count = gradient.shape[0]
    block_size = factor.shape[1]
    blocks = factor.shape[0] // block_size
    shaped = gradient.reshape(row_count, blocks, block_size)
    factors = factor.astype(jnp.float32).reshape(blocks, block_size, block_size)
    result = jnp.einsum("rbi,bij->rbj", shaped, factors, precision=lax.Precision.HIGHEST)
    return result.reshape(row_count, blocks * block_size)


def shards(
    normed,
    rec_cot,
    conv_out,
    gate_cot,
    rec_weight,
    rec_moment,
    rec_right,
    gate_weight,
    gate_moment,
    gate_left,
    gate_right,
):
    token_count = normed.shape[0]
    columns = normed
    partial_rows = lax.psum_scatter(
        lax.dot_general(
            columns, rec_cot, (((0,), (0,)), ((), ())), preferred_element_type=jnp.float32
        ),
        "fs",
        scatter_dimension=0,
        tiled=True,
    )
    rec_grad = lax.psum(partial_rows, "rep")
    rec_pre = precondition_right(rec_grad, rec_right)
    block_count, own_rows, block_size = gate_weight.shape
    conv_blocks = conv_out.reshape(token_count, block_count, block_size)
    cot_blocks = gate_cot.reshape(token_count, block_count, block_size)
    gate_term = jnp.einsum(
        "tbi,tbj->bij", conv_blocks, cot_blocks, preferred_element_type=jnp.float32
    )
    right_factor = gate_right.astype(jnp.float32)
    left_factor = gate_left.astype(jnp.float32)
    part_grad = lax.psum_scatter(gate_term, "fs", scatter_dimension=1, tiled=True)
    gate_grad = lax.psum(part_grad, "rep")
    right_done = jnp.einsum(
        "bij,bjk->bik", gate_grad, right_factor, precision=lax.Precision.HIGHEST
    )
    columns = left_factor
    gate_pre = jnp.einsum(
        "bri,bik->brk",
        columns,
        lax.all_gather(right_done, "fs", axis=1, tiled=True),
        precision=lax.Precision.HIGHEST,
    )
    rec_moment_new = BETA * rec_moment + rec_pre
    gate_moment_new = BETA * gate_moment + gate_pre
    totals = lax.psum(
        (
            jnp.sum(rec_grad * rec_grad),
            jnp.sum(rec_moment_new * rec_moment_new),
            jnp.sum(gate_grad * gate_grad),
            jnp.sum(gate_moment_new * gate_moment_new),
        ),
        ("fs", "tp"),
    )
    rec_scale = jnp.sqrt(totals[0]) / jnp.sqrt(totals[1] + EPSILON)
    gate_scale = jnp.sqrt(totals[2]) / jnp.sqrt(totals[3] + EPSILON)
    rec_taken = LEARN_RATE * rec_scale * rec_moment_new
    gate_taken = LEARN_RATE * gate_scale * gate_moment_new
    rec_new = rec_weight - rec_taken
    gate_new = gate_weight - gate_taken
    return (
        rec_new,
        rec_moment_new,
        rec_taken,
        rec_new.astype(jnp.bfloat16),
        gate_new,
        gate_moment_new,
        gate_taken,
        gate_new.astype(jnp.bfloat16),
    )


def solution(mesh):
    in_specs = (
        P(("fs", "rep"), None),
        P(("fs", "rep"), "tp"),
        P(("fs", "rep"), "tp"),
        P(("fs", "rep"), "tp"),
        P("fs", "tp"),
        P("fs", "tp"),
        P("tp", None),
        P("tp", "fs", None),
        P("tp", "fs", None),
        P("tp", "fs", None),
        P("tp", None, None),
    )
    out_specs = (
        P("fs", "tp"),
        P("fs", "tp"),
        P("fs", "tp"),
        P("fs", "tp"),
        P("tp", "fs", None),
        P("tp", "fs", None),
        P("tp", "fs", None),
        P("tp", "fs", None),
    )
    return jax.shard_map(shards, mesh=mesh, in_specs=in_specs, out_specs=out_specs, check_vma=False)
```

profile of v0, /device:TPU:0, one launch (start us, length us, event | category | flops | bytes accessed | tf_op | source)
XLA Modules:
  0.0 330.2 jit_solution(16885048392378607039)
XLA Ops:
  7.2 0.0 copy-start
  7.2 0.0 reduce-scatter.5.cloned.1.call-start
  7.2 2.6 copy.25
  9.8 3.3 fusion.3
  13.1 0.0 reduce-scatter.5.cloned.1.call-update
  13.1 0.0 reduce-scatter.3.cloned.1.call-start
  13.1 0.0 copy-done
  13.1 7.0 %fusion.9 = f32[2048,1024]{1,0:T(8,128)} fusion(bf16[640,2048]{1,0:T(8,128)(2,1)S(1)} %copy-done, bf16[640,1024]{1,0:T(8,128)(2,1)} %param.12), kind=kOutput, calls=%fused_computation.17 | convolution fusion | flops 2684354560 | bytes 12320768 | tf_op jit(solution)/shard_map/dot_general | solution.py:37
  20.1 0.0 reduce-scatter.3.cloned.1.call-update
  20.2 0.0 copy-start.3
  20.2 0.0 all-reduce.4.cloned.1.call-start
  20.2 23.0 %reduce-scatter.5.cloned.1.call-done = f32[4,64,256]{2,1,0:T(8,128)} async-done(((f32[4,256,256]{2,1,0:T(8,128)}), f32[4,64,256]{2,1,0:T(8,128)}) %reduce-scatter.5.cloned.1.call-update) | async-done | bytes 262160 | tf_op jit(solution)/shard_map/reduce_scatter | solution.py:54
  43.2 145.5 %reduce-scatter.3.cloned.1.call-done = f32[512,1024]{1,0:T(8,128)} async-done(((f32[2048,1024]{1,0:T(8,128)}), f32[512,1024]{1,0:T(8,128)}) %reduce-scatter.3.cloned.1.call-update) | async-done | bytes 2097168 | tf_op jit(solution)/shard_map/reduce_scatter | solution.py:36
  188.8 0.0 all-reduce.4.cloned.1.call-update
  188.8 0.0 all-gather.2.cloned.1.call-start
  188.8 77.6 %all-reduce.4.cloned.1.call-done = (f32[512,1024]{1,0:T(8,128)}, f32[4,64,256]{2,1,0:T(8,128)}) async-done(((f32[512,1024]{1,0:T(8,128)}, f32[4,64,256]{2,1,0:T(8,128)}), (f32[512,1024]{1,0:T(8,128)}, f32[4,64,256]{2,1,0:T(8,128)})) %all-reduce.4.cloned.1.call-update) | async-done | bytes 2359312 | tf_op jit(solution)/shard_map/psum | solution.py:44
  266.5 2.2 fusion.10
  268.7 0.0 all-gather.2.cloned.1.call-update
  268.7 0.0 copy-done.3
  268.7 4.1 %fusion = f32[4,512,256]{1,2,0:T(8,128)} fusion(bf16[4,256,256]{2,1,0:T(8,128)(2,1)S(1)} %bitcast.29, f32[64,4,8,256]{3,2,1,0:T(8,128)} %bitcast.25), kind=kOutput, calls=%fused_computation | convolution fusion | flops 1610612736 | bytes 4718592 | tf_op jit(solution)/shard_map/rbi,bij->rbj/dot_general | solution.py:17
  272.8 0.0 copy-start.2
  272.8 2.9 copy.21
  275.8 0.0 copy-done.2
  275.8 0.7 multiply_reduce_fusion.3
  276.4 0.0 copy-start.4
  276.4 0.0 copy-start.6
  276.4 5.7 %multiply_reduce_fusion = (f32[]{:T(128)}, f32[512,1024]{1,0:T(8,128)}, f32[]{:T(128)}) fusion(f32[512,1024]{1,0:T(8,128)} %copy.21, f32[512,1024]{1,0:T(8,128)} %param.16, f32[512,1024]{1,0:T(8,128)} %get-tuple-element.12), kind=kLoop, calls=%fused_computation.3 | loop fusion | flops 3145726 | bytes 8388616 | tf_op jit(solution)/shard_map/reduce_sum | solution.py:71
  282.1 14.7 %all-gather.2.cloned.1.call-done = f32[4,256,256]{2,1,0:T(8,128)} async-done(((f32[4,64,256]{2,1,0:T(8,128)}), f32[4,256,256]{2,1,0:T(8,128)}) %all-gather.2.cloned.1.call-update) | async-done | bytes 1048592 | tf_op jit(solution)/shard_map/all_gather | solution.py:63
  296.8 0.0 copy-done.4
  296.8 0.0 copy-done.6
  296.8 2.4 multiply_reduce_fusion.2
  299.2 0.0 copy-start.1
  299.2 15.3 %all-reduce = (f32[]{:T(128)}, f32[]{:T(128)}, f32[]{:T(128)}, f32[]{:T(128)}) all-reduce(f32[]{:T(128)} %get-tuple-element.24, f32[]{:T(128)} %get-tuple-element.20, f32[]{:T(128)} %multiply_reduce_fusion.3, f32[]{:T(128)} %get-tuple-element.22), channel_id=1, replica_groups=mesh['fs'=4,'rep'=4,'tp'=2] {'fs','tp'}, use_global_device_ids=true, to_apply=%region_3.0 | all-reduce | flops 4 | bytes 32 | tf_op jit(solution)/shard_map/psum | solution.py:68
  317.3 0.0 copy-start.5
  317.3 5.5 %fusion.8 = (bf16[512,1024]{1,0:T(8,128)(2,1)}, f32[512,1024]{1,0:T(8,128)}, f32[512,1024]{1,0:T(8,128)}) fusion(f32[512,1024]{1,0:T(8,128)} %param.15, f32[512,1024]{1,0:T(8,128)} %get-tuple-element.21, f32[]{:T(128)S(6)} %mul.46), kind=kLoop, calls=%fused_computation.16 | loop fusion | flops 1572864 | bytes 9437188 | tf_op jit(solution)/shard_map/convert_element_type | solution.py:87
  322.8 0.0 copy-done.1
  322.8 0.0 copy-done.5
  322.8 0.9 fusion.7
Async XLA Ops:
  7.2 6.0 %copy-start = (bf16[640,2048]{1,0:T(8,128)(2,1)S(1)}, bf16[640,2048]{1,0:T(8,128)(2,1)}, u32[]{:S(2)}) copy-start(bf16[640,2048]{1,0:T(8,128)(2,1)} %param.11) | copy-start | bytes 7864324
  7.2 36.1 %reduce-scatter.5.cloned.1.call-start = ((), (), s32[]{:S(2)}) async-start(), calls=%async_computation.3 | async-start | bytes 1310720 | tf_op jit(solution)/shard_map/reduce_scatter | solution.py:54
  13.1 175.7 %reduce-scatter.3.cloned.1.call-start = ((), (), s32[]{:S(2)}) async-start(), calls=%async_computation.2 | async-start | bytes 10485760 | tf_op jit(solution)/shard_map/reduce_scatter | solution.py:36
  20.2 248.5 %copy-start.3 = (bf16[1024,256]{1,0:T(8,128)(2,1)S(1)}, bf16[1024,256]{1,0:T(8,128)(2,1)}, u32[]{:S(2)}) copy-start(bf16[1024,256]{1,0:T(8,128)(2,1)} %param.17) | copy-start | bytes 1572868
  20.2 246.3 %all-reduce.4.cloned.1.call-start = ((), (), s32[]{:S(2)}) async-start(), calls=%async_computation.5 | async-start | bytes 4718592 | tf_op jit(solution)/shard_map/psum | solution.py:44
  188.8 108.1 %all-gather.2.cloned.1.call-start = ((), (), s32[]{:S(2)}) async-start(), calls=%async_computation.4 | async-start | bytes 1310720 | tf_op jit(solution)/shard_map/all_gather | solution.py:63
  272.8 2.9 copy-start.2
  276.4 20.4 %copy-start.4 = (f32[4,64,256]{2,1,0:T(8,128)S(1)}, f32[4,64,256]{2,1,0:T(8,128)}, u32[]{:S(2)}) copy-start(f32[4,64,256]{2,1,0:T(8,128)} %param.19) | copy-start | bytes 786436
  276.4 20.4 %copy-start.6 = (bf16[4,64,256]{2,1,0:T(8,128)(2,1)S(1)}, bf16[4,64,256]{2,1,0:T(8,128)(2,1)}, u32[]{:S(2)}) copy-start(bf16[4,64,256]{2,1,0:T(8,128)(2,1)} %param.20) | copy-start | bytes 393220
  299.2 23.6 %copy-start.1 = (f32[4,64,256]{2,1,0:T(8,128)}, f32[4,64,256]{2,1,0:T(8,128)S(1)}, u32[]{:S(2)}) copy-start(f32[4,64,256]{2,1,0:T(8,128)S(1)} %get-tuple-element.23) | copy-start | bytes 786436
  317.3 5.5 %copy-start.5 = (f32[4,64,256]{2,1,0:T(8,128)S(1)}, f32[4,64,256]{2,1,0:T(8,128)}, u32[]{:S(2)}) copy-start(f32[4,64,256]{2,1,0:T(8,128)} %param.18) | copy-start | bytes 786436
Sparse Core Ops, SparseCore 0:
  13.2 29.9 reduce-scatter.4
  45.6 143.1 reduce-scatter.2
  191.9 74.4 all-reduce.3
  268.8 27.9 all-gather.1
where the time goes:
time: 331 us; the launch traced here: 330 us
  waiting for transfers between devices  261 us (79%)
  matrix products  19 us (6%)
  between operations  16.6 us (5%)
  blocking collectives  15.3 us (5%)
  other arithmetic  12.7 us (4%)
  local copies, waits for them, and re-layouts  5.54 us (2%)
    reduce_scatter x1, waiting for transfers between devices, shards(): lax.psum_scatter(lax.dot_general(columns, rec_cot, (((0,), (0,)), ((), ()...  146 us
    psum x1, waiting for transfers between devices, shards(): rec_grad = lax.psum(partial_rows, 'rep')  77.6 us
    reduce_scatter x1, waiting for transfers between devices, shards(): lax.psum_scatter(gate_term, 'fs', scatter_dimension=1, tiled=True)  23 us
    psum x1, blocking collectives, shards(): lax.psum((jnp.sum(rec_grad * rec_grad), jnp.sum(rec_moment_new * rec_mome...  15.3 us
    all_gather x1, waiting for transfers between devices, shards(): lax.all_gather(right_done, 'fs', axis=1, tiled=True)  14.7 us
    dot_general x1, matrix products, shards(): lax.dot_general(columns, rec_cot, (((0,), (0,)), ((), ())), preferred_ele...  7 us
  transfers between devices with their start and end apart: 4, of which 4 were waited for; matrix products, arithmetic and copies ran while one was open for 6% of the time, Pallas kernels for 0%

commit v1 on v0

v1 whole, which is shorter than its diff:
```python
import functools

import jax
import jax.numpy as jnp
from jax import lax
from jax.experimental import pallas as pl
from jax.experimental.pallas import tpu as pltpu
from jax.sharding import PartitionSpec as P

BETA = 0.9
LEARN_RATE = 0.02
EPSILON = 1e-06
MESH = pl.DeviceIdType.MESH
LANES = 128


def split_dot(value, factor):
    high = value.astype(jnp.bfloat16)
    low = (value - high.astype(jnp.float32)).astype(jnp.bfloat16)
    return jnp.dot(high, factor, preferred_element_type=jnp.float32) + jnp.dot(
        low, factor, preferred_element_type=jnp.float32
    )


def split_dot_left(factor, value):
    high = value.astype(jnp.bfloat16)
    low = (value - high.astype(jnp.float32)).astype(jnp.bfloat16)
    return jnp.dot(factor, high, preferred_element_type=jnp.float32) + jnp.dot(
        factor, low, preferred_element_type=jnp.float32
    )


def token_dot(left, right):
    return lax.dot_general(left, right, (((0,), (0,)), ((), ())), preferred_element_type=jnp.float32)


def folded_squares(value):
    squares = value * value
    rows, width = squares.shape
    total = jnp.sum(squares.reshape(rows // 8, 8, width), axis=0)
    result = total[:, :LANES]
    for start in range(LANES, width, LANES):
        result = result + total[:, start : start + LANES]
    return result


def kernel(
    fs_size, tp_size, halves,
    normed, rec_cot, conv_out, gate_cot, rec_moment, rec_right, gate_moment, gate_left, gate_right,
    rec_pre, gate_pre, scales,
    part, first, second, along, grad,
    gate_part, gate_first, gate_second, gate_along, gate_grad,
    sums, sums_fs, sums_tp,
    pair_send, pair_recv, fs_send, fs_recv, sum_send, sum_recv,
):
    fs, rep, tp = lax.axis_index("fs"), lax.axis_index("rep"), lax.axis_index("tp")
    bits = (lax.rem(rep, 2), rep // 2)
    partners = (rep + 1 - 2 * bits[0], rep + 2 - 4 * bits[1])
    fs_peers = [lax.rem(fs + step, fs_size) for step in range(1, fs_size)]
    tp_peers = [lax.rem(tp + step, tp_size) for step in range(1, tp_size)]

    barrier = pltpu.get_barrier_semaphore()
    peers = [{"rep": p} for p in partners] + [{"fs": p} for p in fs_peers] + [{"tp": p} for p in tp_peers]
    for peer in peers:
        pl.semaphore_signal(barrier, inc=1, device_id=peer, device_id_type=MESH)

    chunks = part.shape[0]
    width = part.shape[-1]
    quarter = part.shape[-2]
    half_rows = 8 * quarter
    fs_rows = halves * half_rows
    blocks = gate_part.shape[3]
    gate_rows = gate_part.shape[4]
    unit_count = chunks + 1
    sums[...] = jnp.zeros_like(sums)

    def remote(source, target, send, recv, peer):
        return pltpu.make_async_remote_copy(
            src_ref=source, dst_ref=target, send_sem=send, recv_sem=recv,
            device_id=peer, device_id_type=MESH,
        )

    def views(unit):
        if unit == 0:
            return gate_part, gate_first, gate_second, gate_along, gate_grad
        k = unit - 1
        return part.at[k], first.at[k], second.at[k], along.at[k], grad.at[k]

    def mine(stream):
        return bits[stream], bits[1 - stream]

    def pair_copy(unit, stream, stage):
        p, one, two, _, g = views(unit)
        a, b = mine(stream)
        side = stream if stage in (0, 3) else 1 - stream
        if stage == 0:
            source, target = p.at[stream, 1 - a], one.at[stream]
        elif stage == 1:
            source, target = p.at[stream, a, 1 - b], two.at[stream]
        elif stage == 2:
            source = target = g.at[stream, a, b]
        else:
            source = target = g.at[stream, a]
        return remote(
            source, target, pair_send.at[unit, stream, stage], pair_recv.at[unit, stream, stage],
            {"rep": partners[side]},
        )

    def fs_copy(unit, stream, step):
        p, _, _, slots, _ = views(unit)
        a, b = mine(stream)
        peer = fs_peers[step]
        source = p.at[stream, a, b] if unit == 0 else p.at[stream, a, b, peer]
        return remote(
            source, slots.at[stream, step],
            fs_send.at[unit, stream, step], fs_recv.at[unit, stream, step], {"fs": peer},
        )

    def product(unit):
        if unit == 0:
            @pl.loop(0, blocks)
            def _(block):
                columns = pl.ds(pl.multiple_of(block * width, width), width)
                term = token_dot(conv_out[:, columns], gate_cot[:, columns])
                gate_part[:, :, :, block] = term.reshape(2, 2, 2, gate_rows, width)
        else:
            k = unit - 1
            column, half = k // halves, k % halves
            @pl.loop(0, fs_size)
            def _(owner):
                start = pl.multiple_of(owner * fs_rows + half * half_rows, half_rows)
                term = token_dot(
                    normed[:, pl.ds(start, half_rows)], rec_cot[:, column * width : (column + 1) * width]
                )
                part[k, :, :, :, owner] = term.reshape(2, 2, 2, quarter, width)

    def start_pair(unit, stage):
        for stream in range(2):
            pair_copy(unit, stream, stage).start()

    def add_first(unit):
        p, one, _, _, _ = views(unit)
        for stream in range(2):
            pair_copy(unit, stream, 0).wait_recv()
            a, b = mine(stream)
            @pl.loop(0, p.shape[3])
            def _(i):
                for other in range(2):
                    p[stream, a, other, i] += one[stream, other, i]
            pair_copy(unit, stream, 1).start()

    def add_second(unit):
        p, _, two, _, _ = views(unit)
        for stream in range(2):
            pair_copy(unit, stream, 1).wait_recv()
            a, b = mine(stream)
            @pl.loop(0, p.shape[3])
            def _(i):
                p[stream, a, b, i] += two[stream, i]
            for step in range(fs_size - 1):
                fs_copy(unit, stream, step).start()

    def add_along(unit):
        p, _, _, slots, g = views(unit)
        for stream in range(2):
            a, b = mine(stream)
            for step in range(fs_size - 1):
                fs_copy(unit, stream, step).wait_recv()
            total = p[stream, a, b] if unit == 0 else p[stream, a, b, fs]
            for step in range(fs_size - 1):
                total = total + slots[stream, step]
            g[stream, a, b] = total
            pair_copy(unit, stream, 2).start()

    def forward(unit):
        for stream in range(2):
            pair_copy(unit, stream, 2).wait_recv()
            pair_copy(unit, stream, 3).start()

    def finish(unit):
        for stream in range(2):
            pair_copy(unit, stream, 3).wait_recv()
        if unit == 0:
            @pl.loop(0, blocks)
            def _(block):
                gradient = gate_grad[:, :, :, block].reshape(8 * gate_rows, width)
                right_done = split_dot(gradient, gate_right[block])
                pre = split_dot_left(gate_left[block], right_done)
                gate_pre[block] = pre
                moment = BETA * gate_moment[block] + pre
                sums[2] += folded_squares(gradient) * (1.0 / fs_size)
                sums[3] += folded_squares(moment)
        else:
            k = unit - 1
            column, half = k // halves, k % halves
            columns = slice(column * width, (column + 1) * width)
            rows = slice(half * half_rows, (half + 1) * half_rows)
            gradient = grad[k].reshape(half_rows, width)
            pre = split_dot(gradient, rec_right[columns, :])
            rec_pre[rows, columns] = pre
            moment = BETA * rec_moment[rows, columns] + pre
            sums[0] += folded_squares(gradient)
            sums[1] += folded_squares(moment)

    product(0)
    pl.semaphore_wait(barrier, len(peers))
    stages = (None, add_first, add_second, add_along, forward, finish)
    for tick in range(unit_count + 5):
        if tick < unit_count:
            if tick > 0:
                product(tick)
            start_pair(tick, 0)
        for lag in range(1, 6):
            if 0 <= tick - lag < unit_count:
                stages[lag](tick - lag)

    def exchange(slots, axis, axis_peers, base):
        copies = [
            remote(sums, slots.at[i], sum_send.at[base + i], sum_recv.at[base + i], {axis: peer})
            for i, peer in enumerate(axis_peers)
        ]
        for copy in copies:
            copy.start()
        for copy in copies:
            copy.wait()
        total = sums[...]
        for i in range(len(copies)):
            total = total + slots[i]
        return total

    sums[...] = exchange(sums_fs, "fs", fs_peers, 0)
    total = exchange(sums_tp, "tp", tp_peers, fs_size - 1)
    squares = [jnp.sum(total[i], keepdims=True) for i in range(4)]
    rec_scale = jnp.sqrt(squares[0]) / jnp.sqrt(squares[1] + EPSILON)
    gate_scale = jnp.sqrt(squares[2]) / jnp.sqrt(squares[3] + EPSILON)
    scales[0] = jnp.broadcast_to(rec_scale, (8, LANES))
    scales[1] = jnp.broadcast_to(gate_scale, (8, LANES))

    for unit in range(unit_count):
        for stream in range(2):
            for stage in range(4):
                pair_copy(unit, stream, stage).wait_send()
            for step in range(fs_size - 1):
                fs_copy(unit, stream, step).wait_send()


def shards(fs_size, rep_size, tp_size, normed, rec_cot, conv_out, gate_cot, rec_weight, rec_moment,
           rec_right, gate_weight, gate_moment, gate_left, gate_right):
    assert rep_size == 4
    f32 = jnp.float32
    fs_rows, columns = rec_weight.shape
    width = rec_right.shape[1]
    blocks = gate_weight.shape[0]
    halves = 2 if fs_rows % 256 == 0 else 1
    chunks = columns // width * halves
    quarter = fs_rows // (8 * halves)
    gate_rows = gate_right.shape[1] // 8
    units = chunks + 1
    others = fs_size - 1
    vmem = pl.BlockSpec(memory_space=pltpu.VMEM)
    rec_pre, gate_pre, scales = pl.pallas_call(
        functools.partial(kernel, fs_size, tp_size, halves),
        out_shape=(
            jax.ShapeDtypeStruct(rec_weight.shape, f32),
            jax.ShapeDtypeStruct(gate_weight.shape, f32),
            jax.ShapeDtypeStruct((2, 8, LANES), f32),
        ),
        in_specs=[vmem] * 9,
        out_specs=(vmem,) * 3,
        scratch_shapes=[
            pltpu.VMEM((chunks, 2, 2, 2, fs_size, quarter, width), f32),
            pltpu.VMEM((chunks, 2, 2, fs_size, quarter, width), f32),
            pltpu.VMEM((chunks, 2, fs_size, quarter, width), f32),
            pltpu.VMEM((chunks, 2, others, quarter, width), f32),
            pltpu.VMEM((chunks, 2, 2, 2, quarter, width), f32),
            pltpu.VMEM((2, 2, 2, blocks, gate_rows, width), f32),
            pltpu.VMEM((2, 2, blocks, gate_rows, width), f32),
            pltpu.VMEM((2, blocks, gate_rows, width), f32),
            pltpu.VMEM((2, others, blocks, gate_rows, width), f32),
            pltpu.VMEM((2, 2, 2, blocks, gate_rows, width), f32),
            pltpu.VMEM((4, 8, LANES), f32),
            pltpu.VMEM((others, 4, 8, LANES), f32),
            pltpu.VMEM((tp_size - 1, 4, 8, LANES), f32),
            pltpu.SemaphoreType.DMA((units, 2, 4)),
            pltpu.SemaphoreType.DMA((units, 2, 4)),
            pltpu.SemaphoreType.DMA((units, 2, others)),
            pltpu.SemaphoreType.DMA((units, 2, others)),
            pltpu.SemaphoreType.DMA((others + tp_size - 1,)),
            pltpu.SemaphoreType.DMA((others + tp_size - 1,)),
        ],
        compiler_params=pltpu.CompilerParams(
            collective_id=0, has_side_effects=True, vmem_limit_bytes=60 * 1024 * 1024
        ),
    )(normed, rec_cot, conv_out, gate_cot, rec_moment, rec_right, gate_moment, gate_left, gate_right)

    def update(weight, moment, pre, scale):
        moment_new = BETA * moment + pre
        taken = LEARN_RATE * scale * moment_new
        new = weight - taken
        return new, moment_new, taken, new.astype(jnp.bfloat16)

    return update(rec_weight, rec_moment, rec_pre, scales[0, 0, 0]) + update(
        gate_weight, gate_moment, gate_pre, scales[1, 0, 0]
    )


def solution(mesh):
    in_specs = (
        P(("fs", "rep"), None),
        P(("fs", "rep"), "tp"),
        P(("fs", "rep"), "tp"),
        P(("fs", "rep"), "tp"),
        P("fs", "tp"),
        P("fs", "tp"),
        P("tp", None),
        P("tp", "fs", None),
        P("tp", "fs", None),
        P("tp", "fs", None),
        P("tp", None, None),
    )
    out_specs = (P("fs", "tp"),) * 4 + (P("tp", "fs", None),) * 4
    body = functools.partial(shards, mesh.shape["fs"], mesh.shape["rep"], mesh.shape["tp"])
    return jax.shard_map(body, mesh=mesh, in_specs=in_specs, out_specs=out_specs, check_vma=False)
```

time: 331 us -> 145 us (0.44)
  waiting for transfers between devices: 261 us -> 0 us
  Pallas kernels: 0 us -> 134 us
  matrix products: 19 us -> 0 us
  blocking collectives: 15.3 us -> 0 us
  between operations: 16.6 us -> 2.01 us
  other arithmetic: 12.7 us -> 7.26 us
  local copies, waits for them, and re-layouts: 5.54 us -> 1.23 us
    reduce_scatter x2 -> x0, waiting for transfers between devices: 169 us -> none  [the longest x1 146 us: shards(): lax.psum_scatter(lax.dot_general(columns, rec_cot, (((0,), (0,)), ((), ()...]
    pallas_call x0 -> x1, Pallas kernels: none -> 134 us  [shards(): pl.pallas_call(functools.partial(kernel, fs_size, tp_size, halves), out_s...]
    psum x1 -> x0, waiting for transfers between devices: 77.6 us -> none  [shards(): rec_grad = lax.psum(partial_rows, 'rep')]
    dot_general x5 -> x0, matrix products: 19 us -> none  [the longest x1 7 us: shards(): lax.dot_general(columns, rec_cot, (((0,), (0,)), ((), ())), preferred_ele...]
    psum x1 -> x0, blocking collectives: 15.3 us -> none  [shards(): lax.psum((jnp.sum(rec_grad * rec_grad), jnp.sum(rec_moment_new * rec_mome...]
    all_gather x1 -> x0, waiting for transfers between devices: 14.7 us -> none  [shards(): lax.all_gather(right_done, 'fs', axis=1, tiled=True)]
    reduce_sum x2 -> x0, other arithmetic: 6.32 us -> none  [the longest x1 5.65 us: shards(): jnp.sum(rec_moment_new * rec_moment_new)]
    reshape x2 -> x0, local copies, waits for them, and re-layouts: 5.5 us -> none  [the longest x1 2.92 us: precondition_right(): return result.reshape(row_count, blocks * block_size)]
  transfers between devices with their start and end apart: 4 -> 0, of which waited for: 4 -> 0; matrix products, arithmetic and copies ran while one was open for 6% -> 0% of each run, Pallas kernels for 0% -> 0%
where the time goes in v1:
time: 145 us
  Pallas kernels  134 us (92%)
  other arithmetic  7.26 us (5%)
  between operations  2.01 us (1%)
    pallas_call x1, Pallas kernels, shards(): pl.pallas_call(functools.partial(kernel, fs_size, tp_size, halves), out_s...  134 us
    convert_element_type x2, other arithmetic, update(): return (new, moment_new, taken, new.astype(jnp.bfloat16))  7.26 us

profile of v1, /device:TPU:0, one launch (start us, length us, event | category | flops | bytes accessed | tf_op | source)
XLA Modules:
  0.0 144.8 jit_solution(9501858258850238661)
XLA Ops:
  0.6 0.0 copy-start
  0.6 134.3 %shard_map.170 = (f32[512,1024]{1,0:T(8,128)}, f32[4,64,256]{2,1,0:T(8,128)}, f32[2,8,128]{2,1,0:T(8,128)}) custom-call(bf16[640,2048]{1,0:T(8,128)(2,1)} %normed.1, bf16[640,1024]{1,0:T(8,128)(2,1)} %rec_cot.1, bf16[640,1024]{1,0:T(8,128)(2,1)} %conv_out.1, bf16[640,1024]{1,0:T(8,128)(2,1)} %gate_cot.1, f32[512,1024]{1,0:T(8,128)} %rec_moment.1, ...), custom_call_target="tpu_custom_call" | custom-call | tf_op jit(solution)/shard_map/pallas_call | solution.py:261
  134.9 1.2 fusion.2
  136.8 0.0 copy-done
  136.8 0.0 copy-start.1
  136.8 0.0 copy-start.2
  136.8 0.0 copy-start.3
  136.8 6.3 %fusion.1 = (bf16[512,1024]{1,0:T(8,128)(2,1)}, f32[512,1024]{1,0:T(8,128)}, f32[512,1024]{1,0:T(8,128)}, f32[512,1024]{1,0:T(8,128)}) fusion(f32[512,1024]{1,0:T(8,128)} %param.15, f32[]{:T(128)} %bitcast, f32[512,1024]{1,0:T(8,128)} %get-tuple-element.12, f32[512,1024]{1,0:T(8,128)S(1)} %copy-done), kind=kLoop, calls=%fused_computation.5 | loop fusion | flops 2621440 | bytes 13631492 | tf_op jit(solution)/shard_map/convert_element_type | solution.py:300
  143.8 0.0 copy-done.1
  143.8 0.0 copy-done.2
  143.8 0.0 copy-done.3
  143.8 1.0 fusion
Async XLA Ops:
  0.6 136.2 %copy-start = (f32[512,1024]{1,0:T(8,128)S(1)}, f32[512,1024]{1,0:T(8,128)}, u32[]{:S(2)}) copy-start(f32[512,1024]{1,0:T(8,128)} %rec_moment.1) | copy-start | bytes 6291460
  136.8 7.0 %copy-start.1 = (f32[4,64,256]{2,1,0:T(8,128)S(1)}, f32[4,64,256]{2,1,0:T(8,128)}, u32[]{:S(2)}) copy-start(f32[4,64,256]{2,1,0:T(8,128)} %gate_moment.1) | copy-start | bytes 786436
  136.8 7.0 %copy-start.2 = (f32[4,64,256]{2,1,0:T(8,128)S(1)}, f32[4,64,256]{2,1,0:T(8,128)}, u32[]{:S(2)}) copy-start(f32[4,64,256]{2,1,0:T(8,128)} %param.18) | copy-start | bytes 786436
  136.8 7.0 %copy-start.3 = (f32[4,64,256]{2,1,0:T(8,128)S(1)}, f32[4,64,256]{2,1,0:T(8,128)}, u32[]{:S(2)}) copy-start(f32[4,64,256]{2,1,0:T(8,128)} %get-tuple-element.13) | copy-start | bytes 786436

commit v2 on v1

--- a/solution.py
+++ b/solution.py
@@ -205,14 +205,14 @@
     product(0)
     pl.semaphore_wait(barrier, len(peers))
     stages = (None, add_first, add_second, add_along, forward, finish)
-    for tick in range(unit_count + 5):
+    for tick in range(unit_count + 6):
         if tick < unit_count:
             if tick > 0:
                 product(tick)
             start_pair(tick, 0)
         for lag in range(1, 6):
-            if 0 <= tick - lag < unit_count:
-                stages[lag](tick - lag)
+            if 0 <= tick - lag - 1 < unit_count:
+                stages[lag](tick - lag - 1)
 
     def exchange(slots, axis, axis_peers, base):
         copies = [

time: 145 us -> 146 us (level)
  no operation moved by 1% of the time
where the time goes in v2:
time: 146 us
  Pallas kernels  135 us (92%)
  other arithmetic  7.26 us (5%)
  between operations  2.01 us (1%)
    pallas_call x1, Pallas kernels, shards(): pl.pallas_call(functools.partial(kernel, fs_size, tp_size, halves), out_s...  135 us
    convert_element_type x2, other arithmetic, update(): return (new, moment_new, taken, new.astype(jnp.bfloat16))  7.26 us

profile of v2, /device:TPU:0, one launch (start us, length us, event | category | flops | bytes accessed | tf_op | source)
XLA Modules:
  0.0 145.7 jit_solution(11153336044660542004)
XLA Ops:
  0.6 0.0 copy-start
  0.6 135.2 %shard_map.170 = (f32[512,1024]{1,0:T(8,128)}, f32[4,64,256]{2,1,0:T(8,128)}, f32[2,8,128]{2,1,0:T(8,128)}) custom-call(bf16[640,2048]{1,0:T(8,128)(2,1)} %normed.1, bf16[640,1024]{1,0:T(8,128)(2,1)} %rec_cot.1, bf16[640,1024]{1,0:T(8,128)(2,1)} %conv_out.1, bf16[640,1024]{1,0:T(8,128)(2,1)} %gate_cot.1, f32[512,1024]{1,0:T(8,128)} %rec_moment.1, ...), custom_call_target="tpu_custom_call" | custom-call | tf_op jit(solution)/shard_map/pallas_call | solution.py:261
  135.8 1.2 fusion.2
  137.7 0.0 copy-done
  137.7 0.0 copy-start.1
  137.7 0.0 copy-start.2
  137.7 0.0 copy-start.3
  137.7 6.3 %fusion.1 = (bf16[512,1024]{1,0:T(8,128)(2,1)}, f32[512,1024]{1,0:T(8,128)}, f32[512,1024]{1,0:T(8,128)}, f32[512,1024]{1,0:T(8,128)}) fusion(f32[512,1024]{1,0:T(8,128)} %param.15, f32[]{:T(128)} %bitcast, f32[512,1024]{1,0:T(8,128)} %get-tuple-element.12, f32[512,1024]{1,0:T(8,128)S(1)} %copy-done), kind=kLoop, calls=%fused_computation.5 | loop fusion | flops 2621440 | bytes 13631492 | tf_op jit(solution)/shard_map/convert_element_type | solution.py:300
  144.7 0.0 copy-done.1
  144.7 0.0 copy-done.2
  144.7 0.0 copy-done.3
  144.7 1.0 fusion
Async XLA Ops:
  0.6 137.0 %copy-start = (f32[512,1024]{1,0:T(8,128)S(1)}, f32[512,1024]{1,0:T(8,128)}, u32[]{:S(2)}) copy-start(f32[512,1024]{1,0:T(8,128)} %rec_moment.1) | copy-start | bytes 6291460
  137.7 7.0 %copy-start.1 = (f32[4,64,256]{2,1,0:T(8,128)S(1)}, f32[4,64,256]{2,1,0:T(8,128)}, u32[]{:S(2)}) copy-start(f32[4,64,256]{2,1,0:T(8,128)} %gate_moment.1) | copy-start | bytes 786436
  137.7 7.0 %copy-start.2 = (f32[4,64,256]{2,1,0:T(8,128)S(1)}, f32[4,64,256]{2,1,0:T(8,128)}, u32[]{:S(2)}) copy-start(f32[4,64,256]{2,1,0:T(8,128)} %param.18) | copy-start | bytes 786436
  137.7 7.0 %copy-start.3 = (f32[4,64,256]{2,1,0:T(8,128)S(1)}, f32[4,64,256]{2,1,0:T(8,128)}, u32[]{:S(2)}) copy-start(f32[4,64,256]{2,1,0:T(8,128)} %get-tuple-element.13) | copy-start | bytes 786436
